TPU v7x, 512 devices: a whole 4x4x16 slice. The times are simulated.
512 devices in a mesh: sp: 16 (over z), fs: 4 (over y), tp: 8 (over x, core).
Axes of the slice: x: 4, y: 4, z: 16, core: 2. Of those that a mesh axis runs over, the one named last changes fastest.
Arguments:
- inputs: bfloat16 [4, 8192, 2048], P('fs', 'sp', 'tp'), may hold values from -6 to 6
- norm_gain: float32 [2048], replicated, may hold values from 0.1 to 1.9
- query_weight: bfloat16 [2048, 1024], P(('sp', 'fs'), 'tp'), may hold values from -0.125 to 0.125
- key_weight: bfloat16 [2048, 1024], P(('sp', 'fs'), 'tp'), may hold values from -0.125 to 0.125
- value_weight: bfloat16 [2048, 1024], P(('sp', 'fs'), 'tp'), may hold values from -0.125 to 0.125
- query_gain: float32 [64], replicated, may hold values from 0.8 to 7
- key_gain: float32 [64], replicated, may hold values from 0.8 to 7
- mix_lambda: float32 [8], replicated, may hold values from 0.3 to 0.8
- head_gain: float32 [128], replicated, may hold values from 0.1 to 1.9
- post_gate_weight: bfloat16 [2048, 2048], P(('sp', 'fs'), 'tp'), may hold values from -0.125 to 0.125
- pre_gate_weight: bfloat16 [2048, 2048], P(('sp', 'fs'), 'tp'), may hold values from -0.125 to 0.125
- inner_weight: bfloat16 [2048, 2048], P(('sp', 'fs'), 'tp'), may hold values from -0.125 to 0.125
- conv_taps: float32 [3, 2048], replicated, may hold values from -3 to 3
- attn_out_weight: bfloat16 [2048, 1024], P(('sp', 'fs'), 'tp'), may hold values from -0.109375 to 0.109375
- conv_out_weight: bfloat16 [2048, 2048], P(('sp', 'fs'), 'tp'), may hold values from -0.109375 to 0.109375
Outputs:
- mixed: bfloat16 [4, 8192, 2048], P('fs', ('sp', 'tp'))
All inputs are finite; a program needn't handle non-finite values.
Results may differ from a plain program's by a relative error of at most 0.015.
The roundings to bfloat16 on the way count: a program that leaves them out, or rounds other values in their place, can miss the bound.
Values may be sent and summed in bfloat16 or wider, within the bound.
A program may use at most 64 MiB of HBM per device.

v0:
```python
import math

import jax
import jax.numpy as jnp
from jax import lax
from jax.sharding import PartitionSpec as P

epsilon = 1e-06


def in_one_piece(arrays, axis, dim, along):
    ends, at = ([], 0)
    for a in arrays[:-1]:
        at += a.shape[along]
        ends.append(at)
    both = jnp.concatenate(arrays, axis=along)
    return tuple(jnp.split(lax.all_gather(both, axis, axis=dim, tiled=True), ends, axis=along))


def padded_2(x, sides, width):
    for axis, dim in sides:
        size, length = (lax.axis_size(axis), x.shape[dim])
        up = [(i, (i + 1) % size) for i in range(size - 1)]
        down = [(j, i) for i, j in up]
        last = lax.slice_in_dim(x, length - width, length, axis=dim)
        initial = lax.slice_in_dim(x, 0, width, axis=dim)
        before = lax.ppermute(last, axis, up)
        after = lax.ppermute(initial, axis, down)
        x = jnp.concatenate([before, x, after], axis=dim)
    return x


def in_order(tiles, dim):
    tiles = jnp.moveaxis(tiles, 0, dim)
    lengths = tiles.shape
    return tiles.reshape(*lengths[:dim], lengths[dim] * lengths[dim + 1], *lengths[dim + 2 :])


def from_everyone(x, axis):
    copies = jnp.broadcast_to(x, (lax.axis_size(axis), *x.shape))
    return lax.all_to_all(copies, axis, split_axis=0, concat_axis=0, tiled=True)


def gather_directly(x, axis, dim):
    return in_order(from_everyone(x, axis), dim)


def cut_along(x, dim, length):
    before, after = (x.shape[:dim], x.shape[dim + 1 :])
    return jnp.moveaxis(x.reshape(*before, length, -1, *after), dim, 0)


def summed_on_arrival(x, axis, dim):
    tiles = cut_along(x, dim, lax.axis_size(axis))
    arrived = lax.all_to_all(tiles, axis, split_axis=0, concat_axis=0, tiled=True)
    return arrived.astype(jnp.float32).sum(axis=0)


def scale_rows(values, gain):
    return values * lax.rsqrt(jnp.mean(values * values, axis=-1, keepdims=True) + epsilon) * gain


def project_all(normed, weights, products):
    result = []
    for member in range(len(weights)):
        if member < products:
            result.append(jnp.dot(normed, weights[member], preferred_element_type=jnp.float32))
        else:
            result.append(weights[member])
    return tuple(result)


def attention_branch(query, key, values, weight_two, query_gain, key_gain, head_gain):
    tok_rows = query.shape[0]
    vsize = head_gain.shape[0]
    half = query_gain.shape[0]
    heads = values.shape[1] // vsize
    query_normed = scale_rows(query.reshape(tok_rows, heads, 2, half), query_gain).astype(
        jnp.bfloat16
    )
    key_normed = scale_rows(key.reshape(tok_rows, heads * 2, half), key_gain).astype(jnp.bfloat16)
    key_normed = key_normed.reshape(tok_rows, heads * 2 * half)
    scale = half ** (-0.5)
    initial = (
        jnp.full((heads, 2, tok_rows), -1e30, jnp.float32),
        jnp.zeros((heads, 2, tok_rows), jnp.float32),
        jnp.zeros((heads, 2, tok_rows, vsize), jnp.float32),
    )
    carry = initial
    key_piece, value_piece = in_one_piece((key_normed, values), "sp", 0, 1)
    length = key_piece.shape[0]
    block = math.gcd(length, 512)
    key_blocks = key_piece.reshape(length // block, block, heads, 2, half)
    value_blocks = value_piece.reshape(length // block, block, heads, vsize)

    def one_block(state, blocks):
        peak, total, accum = state
        key_block, value_block = blocks
        scores = (
            jnp.einsum(
                "qhjd,khjd->hjqk", query_normed, key_block, preferred_element_type=jnp.float32
            )
            * scale
        )
        new_peak = jnp.maximum(peak, jnp.max(scores, axis=-1))
        factor = jnp.exp(peak - new_peak)
        expo = jnp.exp(scores - new_peak[..., None])
        total = total * factor + jnp.sum(expo, axis=-1)
        accum = accum * factor[..., None] + jnp.einsum(
            "hjqk,khd->hjqd",
            expo.astype(jnp.bfloat16),
            value_block,
            preferred_element_type=jnp.float32,
        )
        return ((new_peak, total, accum), None)

    carry, unused = lax.scan(one_block, carry, (key_blocks, value_blocks))
    peak, total, accum = carry
    mapped = accum / total[..., None]
    head_out = mapped[:, 0] - weight_two[:, None, None] * mapped[:, 1]
    normed_out = scale_rows(head_out, head_gain).astype(jnp.bfloat16)
    return jnp.transpose(normed_out, (1, 0, 2)).reshape(tok_rows, heads * vsize)


def per_device(
    inputs,
    norm_gain,
    query_weight,
    key_weight,
    value_weight,
    query_gain,
    key_gain,
    mix_lambda,
    head_gain,
    post_gate_weight,
    pre_gate_weight,
    inner_weight,
    conv_taps,
    attn_out_weight,
    conv_out_weight,
):
    tokens = inputs[0]
    tok_rows = tokens.shape[0]
    tokens = padded_2(tokens, (("sp", 0),), 1)
    whole = gather_directly(tokens, "tp", 1)
    normed = scale_rows(whole.astype(jnp.float32), norm_gain).astype(jnp.bfloat16)
    margin = (normed.shape[0] - tok_rows) // 2
    heads_dev = value_weight.shape[1] // head_gain.shape[0]
    channels = post_gate_weight.shape[1]
    tp_index = lax.axis_index("tp")
    weight_two = lax.dynamic_slice_in_dim(mix_lambda, tp_index * heads_dev, heads_dev)
    taps = lax.dynamic_slice_in_dim(conv_taps, tp_index * channels, channels, 1)
    every_full = in_one_piece(
        (
            query_weight,
            key_weight,
            value_weight,
            post_gate_weight,
            pre_gate_weight,
            inner_weight,
            attn_out_weight,
            conv_out_weight,
        ),
        ("sp", "fs"),
        0,
        1,
    )
    query, key, value_proj, post, pre_gate, inner, attn_out_full, conv_out_full = project_all(
        normed, every_full[0:3] + every_full[3:6] + every_full[6:8], 6
    )
    attn_hidden = attention_branch(
        query[margin : margin + tok_rows],
        key[margin : margin + tok_rows],
        value_proj[margin : margin + tok_rows].astype(jnp.bfloat16),
        weight_two,
        query_gain,
        key_gain,
        head_gain,
    )
    post_mid = post[margin : margin + tok_rows].astype(jnp.bfloat16)
    post_wide = lax.optimization_barrier(post_mid).astype(jnp.float32)
    signal = (pre_gate * inner).astype(jnp.bfloat16)
    shifted = lax.optimization_barrier(signal).astype(jnp.float32)
    filtered = taps[0] * shifted[:-2] + taps[1] * shifted[1:-1] + taps[2] * shifted[2:]
    conv_hidden = (post_wide * filtered).astype(jnp.bfloat16)
    contract = (((1,), (1,)), ((), ()))
    summed = summed_on_arrival(
        (
            lax.dot_general(
                attn_hidden, attn_out_full, contract, preferred_element_type=jnp.float32
            )
            + lax.dot_general(
                conv_hidden, conv_out_full, contract, preferred_element_type=jnp.float32
            )
        ).astype(jnp.bfloat16),
        "tp",
        0,
    )
    return summed.astype(jnp.bfloat16)[None]


def solution(mesh):
    placed = (
        P("fs", "sp", "tp"),
        P(),
        P(("sp", "fs"), "tp"),
        P(("sp", "fs"), "tp"),
        P(("sp", "fs"), "tp"),
        P(),
        P(),
        P(),
        P(),
        P(("sp", "fs"), "tp"),
        P(("sp", "fs"), "tp"),
        P(("sp", "fs"), "tp"),
        P(),
        P(("sp", "fs"), "tp"),
        P(("sp", "fs"), "tp"),
    )
    return jax.shard_map(
        per_device,
        mesh=mesh,
        in_specs=placed,
        out_specs=P("fs", ("sp", "tp"), None),
        check_vma=False,
    )
```

profile of v0, /device:TPU:1, one launch (start us, length us, event | category | flops | bytes accessed | tf_op | source)
XLA Modules:
  0.0 353.8 jit_solution(16222251347676328049)
XLA Ops:
  13.6 4.3 %collective-permute-start = (bf16[1,256]{1,0:T(2,128)(2,1)S(1)}, bf16[1,256]{1,0:T(2,128)(2,1)S(1)}, u32[]{:S(2)}, u32[]{:S(2)}) collective-permute-start(bf16[1,256]{1,0:T(2,128)(2,1)S(1)} %get-tuple-element.110), channel_id=1, source_target_pairs={{0,32},{32,64},{64,96},{96,128},{128,160},{160,192},{192,224},{224... | collective-permute-start | bytes 1544 | tf_op jit(solution)/shard_map/ppermute | solution.py:27
  19.3 3.2 collective-permute-done.1
  25.0 8.4 %all-to-all-start = ((bf16[8,514,256]{2,1,0:T(8,128)(2,1)}), bf16[8,514,256]{2,1,0:T(8,128)(2,1)S(1)}, u32[]{:S(2)}, u32[]{:S(2)}) async-start(bf16[8,514,256]{2,1,0:T(8,128)(2,1)} %broadcast_in_dim.15), calls=%async_computation | async-start | bytes 4259840 | tf_op jit(solution)/shard_map/all_to_all | solution.py:41
  33.4 26.5 %all-to-all-done = bf16[8,514,256]{2,1,0:T(8,128)(2,1)S(1)} async-done(((bf16[8,514,256]{2,1,0:T(8,128)(2,1)}), bf16[8,514,256]{2,1,0:T(8,128)(2,1)S(1)}, u32[]{:S(2)}, u32[]{:S(2)}) %all-to-all-start) | async-done | bytes 2105376 | tf_op jit(solution)/shard_map/all_to_all | solution.py:41
  61.9 2.0 copy.28
  65.0 95.9 %all-gather.3.cloned.1.call-done = bf16[2048,1536]{1,0:T(8,128)(2,1)} async-done(((bf16[32,1536]{1,0:T(8,128)(2,1)}), bf16[2048,1536]{1,0:T(8,128)(2,1)}) %all-gather.3.cloned.1.call-update) | async-done | bytes 6291472 | tf_op jit(solution)/shard_map/all_gather | solution.py:17
  160.9 1.9 bitcast_reduce_fusion.1
  162.8 2.0 fusion.36
  167.4 1.9 fusion.26
  169.3 1.9 fusion.22
  171.3 1.9 fusion.28
  173.3 1.9 fusion.18
  175.4 4.0 %fusion.23 = f32[512,2048]{1,0:T(8,128)} fusion(bf16[2048,1536]{1,0:T(8,128)(2,1)} %all-gather.3.cloned.1.call-done, f32[514,256]{1,0:T(8,128)S(1)} %convert_element_type.70, bf16[512,256]{1,0:T(8,128)(2,1)S(1)} %slice.116, f32[256]{0:T(256)S(1)} %bitcast.114, f32[256]{0:T(256)S(1)} %bitcast.113, f32[256]{0:T(256)S(1)} %bitcast.112), kind=kOutput, calls=%fused_computation.36 | convolution fusion | flops 537919488 | bytes 7080960 | tf_op jit(solution)/shard_map/dot_general | solution.py:192
  179.4 59.1 %all-gather.5.cloned.1.call-done = bf16[8192,256]{0,1:T(8,128)(2,1)} async-done(((bf16[512,256]{0,1:T(8,128)(2,1)}), bf16[8192,256]{0,1:T(8,128)(2,1)}) %all-gather.5.cloned.1.call-update) | async-done | bytes 4194320 | tf_op jit(solution)/shard_map/all_gather | solution.py:17
  238.5 2.6 fusion.52
  242.0 2.6 copy.24
  244.6 2.5 copy.27
  247.1 54.2 %while.15 = (s32[]{:T(128)}, f32[1,2,512]{2,1,0:T(2,128)S(1)}, f32[1,2,512]{2,1,0:T(2,128)S(1)}, f32[1,2,512,128]{3,2,1,0:T(8,128)S(1)}, bf16[16,512,1,2,64]{1,4...) while((s32[]{:T(128)}, f32[1,2,512]{2,1,0:T(2,128)S(1)}, ...), condition=%wide.region_6.7_spmd.clone, body=%wide.region_3.6_spmd.clone.sunk | while | flops 205920256 | bytes 7799913 | solution.py:117
  258.7 1.5 fusion.66
  262.1 1.5 fusion.66
  265.5 1.5 fusion.66
  268.8 1.5 fusion.66
  302.3 3.8 %add_convert_fusion = bf16[512,2048]{1,0:T(8,128)(2,1)S(1)} fusion(f32[512,2048]{1,0:T(8,128)} %fusion.23, bf16[2048,1536]{1,0:T(8,128)(2,1)} %all-gather.3.cloned.1.call-done, f32[128]{0:T(128)S(1)} %copy-done.3, f32[512]{0:T(512)S(1)} %add_rsqrt_fusion.3, f32[1,2,512,128]{3,2,1,0:T(8,128)S(1)} %broadcast_divide_fusion, f32[]{:T(128)} %bitcast.9), kind=kOutput, calls=%fused_computation.29 | convolution fusion | flops 270860288 | bytes 7343104 | tf_op jit(solution)/shard_map/dot_general | solution.py:189
  306.2 39.7 %all_to_all.10 = bf16[8,64,2048]{2,1,0:T(8,128)(2,1)S(1)} all-to-all(bf16[8,64,2048]{2,1,0:T(8,128)(2,1)S(1)} %bitcast.104), channel_id=1, replica_groups=mesh['sp'=16,'fs'=4,'tp'=8] {'tp'}, dimensions={0} | all-to-all | bytes 4194304 | tf_op jit(solution)/shard_map/all_to_all | solution.py:55
  (148 shorter events, 67.0 us)
Async XLA Ops:
  6.5 154.4 %all-gather.3.cloned.1.call-start = ((), (), s32[]{:S(2)}) async-start(), calls=%async_computation.2 | async-start | bytes 6389760 | tf_op jit(solution)/shard_map/all_gather | solution.py:17
  12.2 0.6 copy-start
  13.6 5.7 %collective-permute-start = (bf16[1,256]{1,0:T(2,128)(2,1)S(1)}, bf16[1,256]{1,0:T(2,128)(2,1)S(1)}, u32[]{:S(2)}, u32[]{:S(2)}) collective-permute-start(bf16[1,256]{1,0:T(2,128)(2,1)S(1)} %get-tuple-element.110), channel_id=1, source_target_pairs={{0,32},{32,64},{64,96},{96,128},{128,160},{160,192},{192,224},{224... | collective-permute-start | bytes 1544 | tf_op jit(solution)/shard_map/ppermute | solution.py:27
  18.0 4.5 %collective-permute-start.1 = (bf16[1,256]{1,0:T(2,128)(2,1)S(1)}, bf16[1,256]{1,0:T(2,128)(2,1)S(1)}, u32[]{:S(2)}, u32[]{:S(2)}) collective-permute-start(bf16[1,256]{1,0:T(2,128)(2,1)S(1)} %get-tuple-element.111), channel_id=1, source_target_pairs={{32,0},{64,32},{96,64},{128,96},{160,128},{192,160},{224,192},{256... | collective-permute-start | bytes 1544 | tf_op jit(solution)/shard_map/ppermute | solution.py:28
  25.0 8.4 %copy-start.4 = (f32[64]{0:T(128)S(1)}, f32[64]{0:T(128)}, u32[]{:S(2)}) copy-start(f32[64]{0:T(128)} %param.23) | copy-start | bytes 772
  25.0 35.0 %all-to-all-start = ((bf16[8,514,256]{2,1,0:T(8,128)(2,1)}), bf16[8,514,256]{2,1,0:T(8,128)(2,1)S(1)}, u32[]{:S(2)}, u32[]{:S(2)}) async-start(bf16[8,514,256]{2,1,0:T(8,128)(2,1)} %broadcast_in_dim.15), calls=%async_computation | async-start | bytes 4259840 | tf_op jit(solution)/shard_map/all_to_all | solution.py:41
  33.3 205.2 %all-gather.5.cloned.1.call-start = ((), (), s32[]{:S(2)}) async-start(), calls=%async_computation.3 | async-start | bytes 4456448 | tf_op jit(solution)/shard_map/all_gather | solution.py:17
  63.9 0.7 copy-start.1
  162.8 3.0 copy-start.5
  173.3 2.0 copy-start.2
  247.1 55.2 %copy-start.3 = (f32[128]{0:T(128)S(1)}, f32[128]{0:T(128)}, u32[]{:S(2)}) copy-start(f32[128]{0:T(128)} %param.25) | copy-start | bytes 1540
Sparse Core Ops, SparseCore 0:
  13.0 147.8 all-gather.2
  165.9 72.5 all-gather.4
where the time goes:
time: 355 us; the launch traced here: 354 us
  waiting for transfers between devices  185 us (52%)
  matrix products  66.5 us (19%)
  blocking collectives  39.7 us (11%)
  local copies, waits for them, and re-layouts  22.7 us (6%)
  starting transfers between devices  14 us (4%)
  between operations  13.7 us (4%)
  other arithmetic  11.7 us (3%)
    all_gather x2, waiting for transfers between devices, in_one_piece(): lax.all_gather(both, axis, axis=dim, tiled=True)  155 us
    all_to_all x1, blocking collectives, summed_on_arrival(): lax.all_to_all(tiles, axis, split_axis=0, concat_axis=0, tiled=True)  39.7 us
    all_to_all x1, waiting for transfers between devices, from_everyone(): return lax.all_to_all(copies, axis, split_axis=0, concat_axis=0, tiled=True)  26.5 us
    dot_general x16, matrix products, one_block(): jnp.einsum('hjqk,khd->hjqd', expo.astype(jnp.bfloat16), value_block, pref...  24.6 us
    dot_general x16, matrix products, one_block(): jnp.einsum('qhjd,khjd->hjqk', query_normed, key_block, preferred_element_...  22.4 us
    unnamed x24, local copies, waits for them, and re-layouts  14.1 us
    dot_general x6, matrix products, project_all(): jnp.dot(normed, weights[member], preferred_element_type=jnp.float32)  11.6 us
    all_to_all x1, starting transfers between devices, from_everyone(): return lax.all_to_all(copies, axis, split_axis=0, concat_axis=0, tiled=True)  8.37 us
  transfers between devices with their start and end apart: 5, of which 4 were waited for; matrix products, arithmetic and copies ran while one was open for 6% of the time, Pallas kernels for 0%

commit v1 on v0

v1 whole, which is shorter than its diff:
```python
import functools

import jax
import jax.numpy as jnp
from jax import lax
from jax.experimental import pallas as pl
from jax.experimental.pallas import tpu as pltpu
from jax.sharding import PartitionSpec as P

EPS = 1e-06
MESH = pl.DeviceIdType.MESH
F32 = jnp.float32
BF16 = jnp.bfloat16
LOG2E = 1.4426950408889634

NZ, NY, NX = 16, 4, 4
CH1, CH2 = 4, 2


def body(
    tok_ref, wq_ref, wk_ref, wv_ref, wpost_ref, wpre_ref, winner_ref, wao_ref, wco_ref,
    ngain_ref, qgain_ref, kgain_ref, hgain_ref, taps_ref, lam_ref,
    out_ref,
    xg, nrm, w0, w1, w2, kb, vb, qb, m_s, l_s, acc_s, hid, sigb, sigf, halo, postb,
    part, pair_in, psum, rel, fin,
    lsem, xss, xrs, zss, zrs, yds, ydr, yfs, yfr, y1ds, y1dr, y1fs, y1fr,
    y2ds, y2dr, y2fs, y2fr, kvs, kvr, hs, hr, rs, rr,
):
    z = lax.axis_index("sp")
    y = lax.axis_index("fs")
    t = lax.axis_index("tp")
    x = t // 2
    c = t % 2

    def zz(i):
        return (i + 2 * NZ) % NZ

    def yy(i):
        return (i + 2 * NY) % NY

    def xx(i):
        return (i + 2 * NX) % NX

    dev_z = ({"sp": zz(z + 1)}, {"sp": zz(z - 1)})
    dev_y = ({"fs": yy(y + 1)}, {"fs": yy(y - 1)})
    dev_x = ({"tp": xx(x + 1) * 2 + c}, {"tp": xx(x - 1) * 2 + c})
    other = x * 2 + (1 - c)
    dev_c = {"tp": other}
    peers = dev_z + dev_y + dev_x + (dev_c,)

    def rc(src, dst, ssem, rsem, dev):
        return pltpu.make_async_remote_copy(
            src_ref=src, dst_ref=dst, send_sem=ssem, recv_sem=rsem,
            device_id=dev, device_id_type=MESH,
        )

    own = (
        (tok_ref, xg.at[t]),
        (wq_ref, w0.at[z, y, :, 0:128]),
        (wk_ref, w0.at[z, y, :, 128:256]),
        (wv_ref, w0.at[z, y, :, 256:384]),
        (wpost_ref, w1.at[z, y, :, 0:256]),
        (wpre_ref, w1.at[z, y, :, 256:512]),
        (winner_ref, w1.at[z, y, :, 512:768]),
        (wao_ref, w2.at[z, y, :, 0:128]),
        (wco_ref, w2.at[z, y, :, 128:384]),
    )
    local = [pltpu.make_async_copy(s, d, lsem.at[i]) for i, (s, d) in enumerate(own)]
    for cp in local:
        cp.start()
    barrier = pltpu.get_barrier_semaphore()
    for dev in peers:
        pl.semaphore_signal(barrier, inc=1, device_id=dev, device_id_type=MESH)

    qb[...] = jnp.zeros_like(qb)
    m_s[...] = jnp.full_like(m_s, -1e30)
    l_s[...] = jnp.zeros_like(l_s)
    acc_s[...] = jnp.zeros_like(acc_s)

    pl.semaphore_wait(barrier, len(peers))

    pending = []

    def go(copy):
        copy.start()
        pending.append(copy)

    ws = (w0, w1, w2)
    zsteps = ((7, 8), (8, 7), (7, 8))

    def z_copy(g, d, s):
        i = zz(z - (s - 1)) if d == 0 else zz(z + (s - 1))
        w = ws[g]
        return rc(w.at[i, y], w.at[i, y], zss.at[g, d, s - 1], zrs.at[g, d, s - 1], dev_z[d])

    def z_wait(g, d, s):
        i = zz(z - s) if d == 0 else zz(z + s)
        w = ws[g]
        rc(w.at[i, y], w.at[i, y], zss.at[g, d, s - 1], zrs.at[g, d, s - 1], dev_z[d]).wait_recv()

    def y0_send(k, i):
        for d in range(2):
            go(rc(w0.at[i, y], w0.at[i, y], yds.at[d, k], ydr.at[d, k], dev_y[d]))

    def y0_forward(k, i):
        for d in range(2):
            col = yy(y - 1) if d == 0 else yy(y + 1)
            rc(w0.at[i, col], w0.at[i, col], yds.at[d, k], ydr.at[d, k], dev_y[d]).wait_recv()
            half = w0.at[i, col, pl.ds(16 * d, 16)]
            go(rc(half, half, yfs.at[d, k], yfr.at[d, k], dev_y[d]))

    def y0_finish(k, i):
        for d in range(2):
            col = yy(y + 2)
            half = w0.at[i, col, pl.ds(16 * d, 16)]
            rc(half, half, yfs.at[d, k], yfr.at[d, k], dev_y[d]).wait_recv()

    def x_send(k, slot, dev, rows=None):
        ref = xg.at[slot] if rows is None else xg.at[slot, rows]
        go(rc(ref, ref, xss.at[k], xrs.at[k], dev))

    def x_wait(k, slot, rows=None):
        ref = xg.at[slot] if rows is None else xg.at[slot, rows]
        rc(ref, ref, xss.at[k], xrs.at[k], dev_c).wait_recv()

    lo, hi = pl.ds(0, 256), pl.ds(256, 256)
    left, right, far = xx(x - 1), xx(x + 1), xx(x + 2)

    local[1].wait()
    local[2].wait()
    local[3].wait()
    for d in range(2):
        go(z_copy(0, d, 1))
    local[0].wait()
    x_send(0, t, dev_x[0])
    x_send(1, t, dev_x[1])
    x_send(2, t, dev_c)
    y0_send(0, z)
    for i in range(4, 9):
        local[i].wait()
    for g in (1, 2):
        for d in range(2):
            go(z_copy(g, d, 1))

    def slabs_of(s):
        result = []
        if zsteps[0][0] >= s:
            result.append((2 * s - 1, zz(z - s)))
        if zsteps[0][1] >= s:
            result.append((2 * s if zsteps[0][0] >= s else 2 * s - 1, zz(z + s)))
        return result

    def x_service_a():
        x_wait(0, left * 2 + c)
        x_send(5, left * 2 + c, dev_x[0], lo)
        x_wait(1, right * 2 + c)
        x_send(6, right * 2 + c, dev_x[1], hi)
        x_send(3, left * 2 + c, dev_c)
        x_send(4, right * 2 + c, dev_c)

    def x_service_b():
        x_wait(5, far * 2 + c, lo)
        x_send(7, far * 2 + c, dev_c, lo)
        x_wait(6, far * 2 + c, hi)
        x_send(8, far * 2 + c, dev_c, hi)

    def x_finish():
        x_wait(2, other)
        x_wait(3, left * 2 + (1 - c))
        x_wait(4, right * 2 + (1 - c))
        x_wait(7, far * 2 + (1 - c), lo)
        x_wait(8, far * 2 + (1 - c), hi)

    def normalize():
        def tile(i, carry):
            rows = pl.ds(pl.multiple_of(i * 32, 32), 32)
            total = jnp.zeros((32, 256), F32)
            for b in range(8):
                v = xg[b, rows, :].astype(F32)
                total = total + v * v
            r = lax.rsqrt(jnp.sum(total, axis=-1, keepdims=True) * (1.0 / 2048) + EPS)
            for b in range(8):
                v = xg[b, rows, :].astype(F32) * r * ngain_ref[:, b * 256 : (b + 1) * 256]
                nrm[rows, b * 256 : (b + 1) * 256] = v.astype(BF16)
            return carry

        lax.fori_loop(0, 16, tile, 0)

    for s in range(1, 9):
        for g in range(3):
            for d in range(2):
                if zsteps[g][d] >= s:
                    z_wait(g, d, s)
                    if zsteps[g][d] > s:
                        go(z_copy(g, d, s + 1))
            if g == 0:
                for k, i in slabs_of(s):
                    y0_send(k, i)
                if s == 2:
                    y0_forward(0, z)
                if s >= 3:
                    for k, i in slabs_of(s - 2):
                        y0_forward(k, i)
        if s == 3:
            x_service_a()
        if s == 5:
            x_service_b()
        if s == 6:
            x_finish()
            normalize()
    for s in (7, 8):
        for k, i in slabs_of(s):
            y0_forward(k, i)

    def yc(w, n, d, k, col, forward):
        span = NZ // n
        if forward:
            return w.at[pl.ds(k * span + d * (span // 2), span // 2), col]
        return w.at[pl.ds(k * span, span), col]

    y_sets = {1: (w1, CH1, y1ds, y1dr, y1fs, y1fr), 2: (w2, CH2, y2ds, y2dr, y2fs, y2fr)}

    def y_direct(g, k, d):
        w, n, ds, dr, _, _ = y_sets[g]
        ref = yc(w, n, d, k, y, False)
        return rc(ref, ref, ds.at[d, k], dr.at[d, k], dev_y[d])

    def y_forward(g, k, d):
        w, n, _, _, fs, fr = y_sets[g]
        ref = yc(w, n, d, k, yy(y - 1) if d == 0 else yy(y + 1), True)
        return rc(ref, ref, fs.at[d, k], fr.at[d, k], dev_y[d])

    def y_direct_wait(g, k, d):
        w, n, ds, dr, _, _ = y_sets[g]
        ref = yc(w, n, d, k, yy(y - 1) if d == 0 else yy(y + 1), False)
        rc(ref, ref, ds.at[d, k], dr.at[d, k], dev_y[d]).wait_recv()

    def y_forward_wait(g, k, d):
        w, n, _, _, fs, fr = y_sets[g]
        ref = yc(w, n, d, k, yy(y + 2), True)
        rc(ref, ref, fs.at[d, k], fr.at[d, k], dev_y[d]).wait_recv()

    for k in range(CH1):
        for d in range(2):
            go(y_direct(1, k, d))

    y0_finish(0, z)
    for s in range(1, 9):
        for k, i in slabs_of(s):
            y0_finish(k, i)

    lane = lax.broadcasted_iota(jnp.int32, (128, 128), 1)
    first = lane < 64

    def half_norm(v, gain):
        sq = v * v
        s1 = jnp.sum(jnp.where(first, sq, 0.0), axis=-1, keepdims=True)
        s2 = jnp.sum(jnp.where(first, 0.0, sq), axis=-1, keepdims=True)
        r = jnp.where(
            first, lax.rsqrt(s1 * (1.0 / 64) + EPS), lax.rsqrt(s2 * (1.0 / 64) + EPS)
        )
        return v * r * gain

    def qkv_tile(i, carry):
        rows = pl.ds(pl.multiple_of(i * 128, 128), 128)
        rows2 = pl.ds(pl.multiple_of(i * 128 + 512, 128), 128)
        qkv = jnp.dot(
            nrm[rows, :], w0[...].reshape(2048, 384), preferred_element_type=F32
        )
        kb[z, rows, :] = half_norm(qkv[:, 128:256], kgain_ref[...]).astype(BF16)
        vb[z, :, rows] = qkv[:, 256:384].T.astype(BF16)
        qt = half_norm(qkv[:, 0:128], qgain_ref[...]).T.astype(BF16)
        qb[0:64, rows] = qt[0:64]
        qb[64:128, rows2] = qt[64:128]
        return carry

    lax.fori_loop(0, 4, qkv_tile, 0)

    bufs = (kb, vb)

    def kv_copy(d, w, s):
        i = zz(z - (s - 1)) if d == 0 else zz(z + (s - 1))
        ref = bufs[w].at[i]
        return rc(ref, ref, kvs.at[d, w, s - 1], kvr.at[d, w, s - 1], dev_z[d])

    def kv_wait(d, w, s):
        i = zz(z - s) if d == 0 else zz(z + s)
        ref = bufs[w].at[i]
        rc(ref, ref, kvs.at[d, w, s - 1], kvr.at[d, w, s - 1], dev_z[d]).wait_recv()

    for w in range(2):
        for d in range(2):
            kv_copy(d, w, 1).start()

    factor = LOG2E * 0.125

    def attend(b):
        def tile(j, carry):
            cols = pl.ds(pl.multiple_of(j * 256, 256), 256)
            st = jnp.dot(kb[b], qb[:, cols], preferred_element_type=F32)
            m_old = m_s[:, cols]
            m_new = jnp.maximum(m_old, jnp.max(st, axis=0, keepdims=True))
            p = jnp.exp2((st - m_new) * factor)
            a = jnp.exp2((m_old - m_new) * factor)
            l_s[:, cols] = l_s[:, cols] * a + jnp.sum(p, axis=0, keepdims=True)
            acc_s[:, cols] = acc_s[:, cols] * a + jnp.dot(
                vb[b], p.astype(BF16), preferred_element_type=F32
            )
            m_s[:, cols] = m_new
            return carry

        lax.fori_loop(0, 4, tile, 0)

    attend(z)

    def conv_project():
        def tile(i, carry):
            rows = pl.ds(pl.multiple_of(i * 128, 128), 128)
            rows8 = pl.ds(pl.multiple_of(i * 128 + 8, 8), 128)
            r = jnp.dot(nrm[rows, :], w1[...].reshape(2048, 768), preferred_element_type=F32)
            postb[rows, :] = r[:, 0:256].astype(BF16)
            signal = (r[:, 256:512] * r[:, 512:768]).astype(BF16)
            sigb[rows, :] = signal
            sigf[rows8, :] = signal.astype(F32)
            return carry

        lax.fori_loop(0, 4, tile, 0)

    def halo_copy(d):
        src = sigb.at[pl.ds(496, 16)] if d == 0 else sigb.at[pl.ds(0, 16)]
        return rc(src, halo.at[d], hs.at[d], hr.at[d], dev_z[d])

    def conv_filter():
        before = halo[0].astype(F32)[8:16]
        after = halo[1].astype(F32)[0:8]
        sigf[0:8, :] = jnp.where(z > 0, before, 0.0)
        sigf[520:528, :] = jnp.where(z < NZ - 1, after, 0.0)
        taps = taps_ref[:, pl.ds(pl.multiple_of(t * 256, 256), 256)]
        for i in range(4):
            r = i * 128
            filtered = (
                taps[0:1] * sigf[r + 7 : r + 135, :]
                + taps[1:2] * sigf[r + 8 : r + 136, :]
                + taps[2:3] * sigf[r + 9 : r + 137, :]
            )
            hid[r : r + 128, 128:384] = (
                postb[r : r + 128, :].astype(F32) * filtered
            ).astype(BF16)

    def kv_step(s, carry):
        for w in range(2):
            for d in range(2):
                kv_wait(d, w, s)
                if d == w:
                    kv_copy(d, w, s + 1).start()
                else:

                    @pl.when(s < 7)
                    def _():
                        kv_copy(d, w, s + 1).start()

        for k in range(CH1):

            @pl.when(s == k + 1)
            def _():
                for d in range(2):
                    y_direct_wait(1, k, d)
                    y_forward(1, k, d).start()

        for k in range(CH2):

            @pl.when(s == k + 3)
            def _():
                for d in range(2):
                    y_direct(2, k, d).start()

            @pl.when(s == k + 6)
            def _():
                for d in range(2):
                    y_direct_wait(2, k, d)
                    y_forward(2, k, d).start()

        attend(zz(z - s))
        attend(zz(z + s))

        @pl.when(s == 6)
        def _():
            for k in range(CH1):
                for d in range(2):
                    y_forward_wait(1, k, d)
            conv_project()
            for d in range(2):
                halo_copy(d).start()

        @pl.when(s == 7)
        def _():
            for d in range(2):
                halo_copy(d).wait_recv()
            conv_filter()

        return carry

    lax.fori_loop(1, 8, kv_step, 0)
    for k in range(CH2):
        for d in range(2):
            y_forward_wait(2, k, d)
    kv_wait(0, 0, 8)
    kv_wait(1, 1, 8)
    attend(zz(z + 8))

    lam = lam_ref[t]
    inv = 1.0 / l_s[...]
    head = acc_s[:, 0:512] * inv[:, 0:512] - lam * (acc_s[:, 512:1024] * inv[:, 512:1024])
    r = lax.rsqrt(jnp.sum(head * head, axis=0, keepdims=True) * (1.0 / 128) + EPS)
    hid[:, 0:128] = ((head * r).T * hgain_ref[...]).astype(BF16)

    def out_tile(n, carry):
        cols = pl.ds(pl.multiple_of(n * 256, 256), 256)
        w = w2[pl.ds(n * 2, 2)].reshape(256, 384)
        r = lax.dot_general(
            hid[...], w, (((1,), (1,)), ((), ())), preferred_element_type=F32
        )
        part[:, :, :, cols] = r.astype(BF16).reshape(NX, 2, 64, 256)
        return carry

    lax.fori_loop(0, 8, out_tile, 0)

    pair = rc(part.at[:, 1 - c], pair_in, rs.at[0], rr.at[0], dev_c)
    pair.start()
    pair.wait_recv()
    up, down = pl.ds(0, 32), pl.ds(32, 32)

    def sum_pair(j):
        psum[j] = (part[j, c].astype(F32) + pair_in[j].astype(F32)).astype(BF16)

    sum_pair(far)
    r1 = rc(psum.at[far, up], rel.at[0], rs.at[1], rr.at[1], dev_x[0])
    r1.start()
    r2 = rc(psum.at[far, down], rel.at[1], rs.at[2], rr.at[2], dev_x[1])
    r2.start()
    sum_pair(right)
    sum_pair(left)
    r3 = rc(psum.at[right, down], fin.at[0, down], rs.at[3], rr.at[3], dev_x[0])
    r3.start()
    r4 = rc(psum.at[left, up], fin.at[1, up], rs.at[4], rr.at[4], dev_x[1])
    r4.start()
    r1.wait_recv()
    psum[right, 0:32] = (psum[right, 0:32].astype(F32) + rel[0].astype(F32)).astype(BF16)
    r5 = rc(psum.at[right, up], fin.at[0, up], rs.at[5], rr.at[5], dev_x[0])
    r5.start()
    r2.wait_recv()
    psum[left, 32:64] = (psum[left, 32:64].astype(F32) + rel[1].astype(F32)).astype(BF16)
    r6 = rc(psum.at[left, down], fin.at[1, down], rs.at[6], rr.at[6], dev_x[1])
    r6.start()
    mine = part[x, c].astype(F32) + pair_in[x].astype(F32)
    for cp in (r3, r4, r5, r6):
        cp.wait_recv()
    out_ref[...] = (mine + fin[0].astype(F32) + fin[1].astype(F32)).astype(BF16)

    for cp in pending:
        cp.wait_send()
    for w in range(2):
        for d in range(2):
            for s in range(1, 9 if d == w else 8):
                kv_copy(d, w, s).wait_send()
    for g, n in ((1, CH1), (2, CH2)):
        for k in range(n):
            for d in range(2):
                if g == 2:
                    y_direct(g, k, d).wait_send()
                y_forward(g, k, d).wait_send()
    for d in range(2):
        halo_copy(d).wait_send()
    for cp in (pair, r1, r2, r3, r4, r5, r6):
        cp.wait_send()


def per_device(
    inputs, norm_gain, query_weight, key_weight, value_weight, query_gain, key_gain,
    mix_lambda, head_gain, post_gate_weight, pre_gate_weight, inner_weight, conv_taps,
    attn_out_weight, conv_out_weight,
):
    hbm = pl.BlockSpec(memory_space=pl.ANY)
    vmem = pl.BlockSpec(memory_space=pltpu.VMEM)
    smem = pl.BlockSpec(memory_space=pltpu.SMEM)
    sem = pltpu.SemaphoreType.DMA
    out = pl.pallas_call(
        body,
        out_shape=jax.ShapeDtypeStruct((64, 2048), BF16),
        in_specs=[hbm] * 9 + [vmem] * 5 + [smem],
        out_specs=vmem,
        scratch_shapes=[
            pltpu.VMEM((8, 512, 256), BF16),
            pltpu.VMEM((512, 2048), BF16),
            pltpu.VMEM((NZ, NY, 32, 384), BF16),
            pltpu.VMEM((NZ, NY, 32, 768), BF16),
            pltpu.VMEM((NZ, NY, 32, 384), BF16),
            pltpu.VMEM((NZ, 512, 128), BF16),
            pltpu.VMEM((NZ, 128, 512), BF16),
            pltpu.VMEM((128, 1024), BF16),
            pltpu.VMEM((1, 1024), F32),
            pltpu.VMEM((1, 1024), F32),
            pltpu.VMEM((128, 1024), F32),
            pltpu.VMEM((512, 384), BF16),
            pltpu.VMEM((512, 256), BF16),
            pltpu.VMEM((528, 256), F32),
            pltpu.VMEM((2, 16, 256), BF16),
            pltpu.VMEM((512, 256), BF16),
            pltpu.VMEM((NX, 2, 64, 2048), BF16),
            pltpu.VMEM((NX, 64, 2048), BF16),
            pltpu.VMEM((NX, 64, 2048), BF16),
            pltpu.VMEM((2, 32, 2048), BF16),
            pltpu.VMEM((2, 64, 2048), BF16),
            sem((9,)),
            sem((9,)),
            sem((9,)),
            sem((3, 2, 8)),
            sem((3, 2, 8)),
            sem((2, 16)),
            sem((2, 16)),
            sem((2, 16)),
            sem((2, 16)),
            sem((2, CH1)),
            sem((2, CH1)),
            sem((2, CH1)),
            sem((2, CH1)),
            sem((2, CH2)),
            sem((2, CH2)),
            sem((2, CH2)),
            sem((2, CH2)),
            sem((2, 2, 8)),
            sem((2, 2, 8)),
            sem((2,)),
            sem((2,)),
            sem((7,)),
            sem((7,)),
        ],
        compiler_params=pltpu.CompilerParams(
            collective_id=0, has_side_effects=True, vmem_limit_bytes=60 * 1024 * 1024
        ),
    )(
        inputs[0], query_weight, key_weight, value_weight, post_gate_weight,
        pre_gate_weight, inner_weight, attn_out_weight, conv_out_weight,
        norm_gain.reshape(1, -1),
        jnp.tile(query_gain, 2).reshape(1, -1),
        jnp.tile(key_gain, 2).reshape(1, -1),
        head_gain.reshape(1, -1),
        conv_taps,
        mix_lambda,
    )
    return out[None]


def solution(mesh):
    rows = P(("sp", "fs"), "tp")
    placed = (
        P("fs", "sp", "tp"), P(), rows, rows, rows, P(), P(), P(), P(),
        rows, rows, rows, P(), rows, rows,
    )
    return jax.shard_map(
        per_device,
        mesh=mesh,
        in_specs=placed,
        out_specs=P("fs", ("sp", "tp"), None),
        check_vma=False,
    )
```

time: 355 us -> 125 us (0.35)
  waiting for transfers between devices: 185 us -> 0 us
  Pallas kernels: 0 us -> 121 us
  matrix products: 66.5 us -> 0 us
  blocking collectives: 39.7 us -> 0 us
  local copies, waits for them, and re-layouts: 22.7 us -> 3.54 us
  starting transfers between devices: 14 us -> 0 us
  between operations: 13.7 us -> 0.01 us
  other arithmetic: 11.7 us -> 0 us
    all_gather x2 -> x0, waiting for transfers between devices: 155 us -> none  [in_one_piece(): lax.all_gather(both, axis, axis=dim, tiled=True)]
    pallas_call x0 -> x1, Pallas kernels: none -> 121 us  [per_device(): pl.pallas_call(body, out_shape=jax.ShapeDtypeStruct((64, 2048), BF16), in...]
    dot_general x40 -> x0, matrix products: 66.5 us -> none  [the longest x16 24.6 us: one_block(): jnp.einsum('hjqk,khd->hjqd', expo.astype(jnp.bfloat16), value_block, pref...]
    all_to_all x1 -> x0, blocking collectives: 39.7 us -> none  [summed_on_arrival(): lax.all_to_all(tiles, axis, split_axis=0, concat_axis=0, tiled=True)]
    all_to_all x1 -> x0, waiting for transfers between devices: 26.5 us -> none  [from_everyone(): return lax.all_to_all(copies, axis, split_axis=0, concat_axis=0, tiled=True)]
    unnamed x24 -> x5, local copies, waits for them, and re-layouts: 14.1 us -> 2.39 us
    all_to_all x1 -> x0, starting transfers between devices: 8.37 us -> none  [from_everyone(): return lax.all_to_all(copies, axis, split_axis=0, concat_axis=0, tiled=True)]
    reduce_sum x20 -> x0, other arithmetic: 8.29 us -> none  [the longest x16 5.83 us: one_block(): total = total * factor + jnp.sum(expo, axis=-1)]
  transfers between devices with their start and end apart: 5 -> 0, of which waited for: 4 -> 0; matrix products, arithmetic and copies ran while one was open for 6% -> 0% of each run, Pallas kernels for 0% -> 0%
where the time goes in v1:
time: 125 us
  Pallas kernels  121 us (97%)
  local copies, waits for them, and re-layouts  3.54 us (3%)
    pallas_call x1, Pallas kernels, per_device(): pl.pallas_call(body, out_shape=jax.ShapeDtypeStruct((64, 2048), BF16), in...  121 us

profile of v1, /device:TPU:1, one launch (start us, length us, event | category | flops | bytes accessed | tf_op | source)
XLA Modules:
  0.0 124.5 jit_solution(17330279626567241451)
XLA Ops:
  0.0 0.0 copy-start
  0.0 0.7 copy-done
  0.7 0.0 copy-start.1
  0.7 0.6 reshape_tile.6.qgain_ref
  1.3 0.1 copy-done.1
  1.3 0.6 reshape_tile.7.kgain_ref
  1.9 121.0 %shard_map.145 = bf16[64,2048]{1,0:T(8,128)(2,1)} custom-call(bf16[512,256]{1,0:T(8,128)(2,1)} %bitcast.5, bf16[32,128]{1,0:T(8,128)(2,1)} %wq_ref.1, bf16[32,128]{1,0:T(8,128)(2,1)} %wk_ref.1, bf16[32,128]{1,0:T(8,128)(2,1)} %wv_ref.1, bf16[32,256]{1,0:T(8,128)(2,1)} %wpost_ref.1, bf16[32,256]{1,0:T(8,128)(2,1)} %wpre_ref.1, bf16[32,256]{1,0:T(8,128)(2,1)} %winner_ref.1, ...), custom_call_target="tpu_custom_call" | custom-call | tf_op jit(solution)/shard_map/pallas_call | solution.py:487
  122.9 1.7 %copy.17 = bf16[1,64,2048]{2,1,0:T(8,128)(2,1)} copy(bf16[1,64,2048]{2,1,0:T(8,128)(2,1)} %bitcast.4) | data formatting | bytes 524288
  (2 shorter events, 0.0 us)
Async XLA Ops:
  0.0 0.7 copy-start
  0.7 0.7 copy-start.1

commit v2 on v1

v2 whole, which is shorter than its diff:
```python
import functools

import jax
import jax.numpy as jnp
from jax import lax
from jax.experimental import pallas as pl
from jax.experimental.pallas import tpu as pltpu
from jax.sharding import PartitionSpec as P

EPS = 1e-06
MESH = pl.DeviceIdType.MESH
F32 = jnp.float32
BF16 = jnp.bfloat16
LOG2E = 1.4426950408889634

NZ, NY, NX = 16, 4, 4


def body(
    tok_ref, wq_ref, wk_ref, wv_ref, wpost_ref, wpre_ref, winner_ref, wao_ref, wco_ref,
    ngain_ref, qgain_ref, kgain_ref, hgain_ref, taps_ref, lam_ref,
    out_ref,
    xg, nrm, w0, wa, w2, w3, kb, vb, qb, m_s, l_s, acc_s, hid, ah, conv, sigb, sigf, halo, postb,
    part, pair_in, psum, rel, fin,
    lsem, xss, xrs, xas, xar, zss, zrs, yds, ydr, yfs, yfr,
    kvs, kvr, hs, hr, rs, rr, als, alr,
):
    z = lax.axis_index("sp")
    y = lax.axis_index("fs")
    t = lax.axis_index("tp")
    x = t // 2
    c = t % 2

    def zz(i):
        return (i + 2 * NZ) % NZ

    def yy(i):
        return (i + 2 * NY) % NY

    def xx(i):
        return (i + 2 * NX) % NX

    dev_z = ({"sp": zz(z + 1)}, {"sp": zz(z - 1)})
    dev_zz = ({"sp": zz(z + 2)}, {"sp": zz(z - 2)})
    dev_y = ({"fs": yy(y + 1)}, {"fs": yy(y - 1)})
    dev_x = ({"tp": xx(x + 1) * 2 + c}, {"tp": xx(x - 1) * 2 + c})
    other = x * 2 + (1 - c)
    dev_c = {"tp": other}
    group = tuple({"tp": (t + i) % 8} for i in range(1, 8))
    peers = dev_z + dev_zz + dev_y + group

    def rc(src, dst, ssem, rsem, dev):
        return pltpu.make_async_remote_copy(
            src_ref=src, dst_ref=dst, send_sem=ssem, recv_sem=rsem,
            device_id=dev, device_id_type=MESH,
        )

    own = (
        (tok_ref, xg.at[t]),
        (wq_ref, w0.at[z, y, :, 0:128]),
        (wk_ref, w0.at[z, y, :, 128:256]),
        (wv_ref, w0.at[z, y, :, 256:384]),
        (wao_ref, wa.at[t, z, y]),
        (wpost_ref, w2.at[z, y, :, 0:256]),
        (wpre_ref, w2.at[z, y, :, 256:512]),
        (winner_ref, w2.at[z, y, :, 512:768]),
        (wco_ref, w3.at[z, y]),
    )
    local = [pltpu.make_async_copy(s, d, lsem.at[i]) for i, (s, d) in enumerate(own)]
    for cp in local:
        cp.start()
    barrier = pltpu.get_barrier_semaphore()
    for dev in peers:
        pl.semaphore_signal(barrier, inc=1, device_id=dev, device_id_type=MESH)

    qb[...] = jnp.zeros_like(qb)
    m_s[...] = jnp.full_like(m_s, -1e30)
    l_s[...] = jnp.zeros_like(l_s)
    acc_s[...] = jnp.zeros_like(acc_s)

    pl.semaphore_wait(barrier, len(peers))

    own_wa = wa.at[t]
    ws = (w0, own_wa, w2, w3)
    zsteps = ((7, 8), (8, 7), (7, 8), (8, 7))

    def z_slab(d, s):
        return zz(z - s) if d == 0 else zz(z + s)

    def z_copy(g, d, s, stride=1):
        ref = ws[g].at[z_slab(d, s - stride), y]
        dev = (dev_z if stride == 1 else dev_zz)[d]
        return rc(ref, ref, zss.at[g, d, s - 1], zrs.at[g, d, s - 1], dev)

    def z_wait(g, d, s):
        ref = ws[g].at[z_slab(d, s), y]
        rc(ref, ref, zss.at[g, d, s - 1], zrs.at[g, d, s - 1], dev_z[d]).wait_recv()

    def z_serve(s):
        for g in (2, 3):
            for d in range(2):
                if s <= zsteps[g][d]:
                    z_wait(g, d, s)
                    if s < zsteps[g][d]:
                        z_copy(g, d, s + 1).start()

    def level(s):
        return (0,) if s == 0 else (15,) if s == 8 else (2 * s - 1, 2 * s)

    def slab_at(k):
        return zz(z + (k + 1) // 2 * (1 - 2 * (k % 2)))

    def y_direct(g, k, d, mine):
        col = y if mine else yy(y - 1) if d == 0 else yy(y + 1)
        ref = ws[g].at[slab_at(k), col]
        return rc(ref, ref, yds.at[g, d, k], ydr.at[g, d, k], dev_y[d])

    def y_half(g, k, d, mine):
        col = yy(y + 2) if not mine else yy(y - 1) if d == 0 else yy(y + 1)
        ref = ws[g].at[slab_at(k), col, pl.ds(16 * d, 16)]
        return rc(ref, ref, yfs.at[g, d, k], yfr.at[g, d, k], dev_y[d])

    def y_send(g, *steps):
        for s in steps:
            for k in level(s):
                for d in range(2):
                    y_direct(g, k, d, True).start()

    def y_relay(g, *steps):
        for s in steps:
            for k in level(s):
                for d in range(2):
                    y_direct(g, k, d, False).wait_recv()
                    y_half(g, k, d, True).start()

    def y_done(g, *steps):
        for s in steps:
            for k in level(s):
                for d in range(2):
                    y_half(g, k, d, False).wait_recv()

    left, right, far = xx(x - 1), xx(x + 1), xx(x + 2)

    def x_gather(buf, lo, hi, ss, sr, start):
        def send(k, slot, dev, piece=None):
            ref = buf.at[slot] if piece is None else buf.at[slot, piece]
            start(rc(ref, ref, ss.at[k], sr.at[k], dev))

        def wait(k, slot, piece=None):
            ref = buf.at[slot] if piece is None else buf.at[slot, piece]
            rc(ref, ref, ss.at[k], sr.at[k], dev_c).wait_recv()

        def begin():
            send(0, t, dev_x[0])
            send(1, t, dev_x[1])
            send(2, t, dev_c)

        def middle():
            wait(0, left * 2 + c)
            send(5, left * 2 + c, dev_x[0], lo)
            wait(1, right * 2 + c)
            send(6, right * 2 + c, dev_x[1], hi)
            send(3, left * 2 + c, dev_c)
            send(4, right * 2 + c, dev_c)

        def late():
            wait(5, far * 2 + c, lo)
            send(7, far * 2 + c, dev_c, lo)
            wait(6, far * 2 + c, hi)
            send(8, far * 2 + c, dev_c, hi)

        def finish():
            wait(2, other)
            wait(3, left * 2 + (1 - c))
            wait(4, right * 2 + (1 - c))
            wait(7, far * 2 + (1 - c), lo)
            wait(8, far * 2 + (1 - c), hi)

        def drain():
            for k, slot, piece in (
                (0, t, None), (1, t, None), (2, t, None),
                (5, left * 2 + c, lo), (6, right * 2 + c, hi),
                (3, left * 2 + c, None), (4, right * 2 + c, None),
                (7, far * 2 + c, lo), (8, far * 2 + c, hi),
            ):
                ref = buf.at[slot] if piece is None else buf.at[slot, piece]
                rc(ref, ref, ss.at[k], sr.at[k], dev_c).wait_send()

        return begin, middle, late, finish, drain

    x_begin, x_service_a, x_service_b, x_finish, x_drain = x_gather(
        xg, pl.ds(0, 256), pl.ds(256, 256), xss, xrs, lambda copy: copy.start()
    )
    a_begin, a_middle, a_late, a_finish, a_drain = x_gather(
        wa, pl.ds(0, 8), pl.ds(8, 8), xas, xar, lambda copy: copy.start()
    )

    for i in (1, 2, 3):
        local[i].wait()
    for stride in (1, 2):
        for d in range(2):
            z_copy(0, d, stride, stride).start()
    local[0].wait()
    x_begin()
    y_send(0, 0)
    local[4].wait()
    for stride in (1, 2):
        for d in range(2):
            z_copy(1, d, stride, stride).start()
    y_send(1, 0)
    for i in range(5, 9):
        local[i].wait()
    for g in (2, 3):
        for d in range(2):
            z_copy(g, d, 1).start()

    def normalize():
        def tile(i, carry):
            rows = pl.ds(pl.multiple_of(i * 32, 32), 32)
            total = jnp.zeros((32, 256), F32)
            for b in range(8):
                v = xg[b, rows, :].astype(F32)
                total = total + v * v
            r = lax.rsqrt(jnp.sum(total, axis=-1, keepdims=True) * (1.0 / 2048) + EPS)
            for b in range(8):
                v = xg[b, rows, :].astype(F32) * r * ngain_ref[:, b * 256 : (b + 1) * 256]
                nrm[rows, b * 256 : (b + 1) * 256] = v.astype(BF16)
            return carry

        lax.fori_loop(0, 16, tile, 0)

    def z_round(r):
        for g in (0, 1):
            for s in (2 * r - 1, 2 * r):
                for d in range(2):
                    if s <= zsteps[g][d]:
                        z_wait(g, d, s)
                        if s + 2 <= zsteps[g][d]:
                            z_copy(g, d, s + 2, 2).start()
                y_send(g, s)

    z_round(1)
    y_relay(0, 0)
    z_serve(1)
    z_round(2)
    y_relay(0, 1, 2)
    y_relay(1, 0)
    z_serve(2)
    x_service_a()
    z_round(3)
    y_relay(0, 3, 4)
    y_relay(1, 1, 2)
    z_serve(3)
    z_round(4)
    y_relay(0, 5, 6)
    x_service_b()
    y_relay(0, 7, 8)
    y_relay(1, 3, 4)
    y_send(2, 0)
    z_serve(4)
    x_finish()
    normalize()
    z_serve(5)
    y_relay(1, 5, 6)
    y_send(2, 1, 2)
    y_done(0, *range(9))

    lane = lax.broadcasted_iota(jnp.int32, (128, 128), 1)
    first = lane < 64

    def half_norm(v, gain):
        sq = v * v
        s1 = jnp.sum(jnp.where(first, sq, 0.0), axis=-1, keepdims=True)
        s2 = jnp.sum(jnp.where(first, 0.0, sq), axis=-1, keepdims=True)
        r = jnp.where(
            first, lax.rsqrt(s1 * (1.0 / 64) + EPS), lax.rsqrt(s2 * (1.0 / 64) + EPS)
        )
        return v * r * gain

    kgain = jnp.concatenate([kgain_ref[...]] * 2, axis=1)
    qgain = jnp.concatenate([qgain_ref[...]] * 2, axis=1)

    def kv_tile(i, carry):
        rows = pl.ds(pl.multiple_of(i * 128, 128), 128)
        kv = jnp.dot(
            nrm[rows, :], w0[:, :, :, 128:384].reshape(2048, 256), preferred_element_type=F32
        )
        kb[z, rows, :] = half_norm(kv[:, 0:128], kgain).astype(BF16)
        vb[z, :, rows] = kv[:, 128:256].T.astype(BF16)
        return carry

    def q_tile(i, carry):
        rows = pl.ds(pl.multiple_of(i * 128, 128), 128)
        rows2 = pl.ds(pl.multiple_of(i * 128 + 512, 128), 128)
        q = jnp.dot(
            nrm[rows, :], w0[:, :, :, 0:128].reshape(2048, 128), preferred_element_type=F32
        )
        qt = half_norm(q, qgain).T.astype(BF16)
        qb[0:64, rows] = qt[0:64]
        qb[64:128, rows2] = qt[64:128]
        return carry

    lax.fori_loop(0, 4, kv_tile, 0)

    bufs = (kb, vb)

    def kv_copy(d, w, s):
        i = zz(z - (s - 1)) if d == 0 else zz(z + (s - 1))
        ref = bufs[w].at[i]
        return rc(ref, ref, kvs.at[d, w, s - 1], kvr.at[d, w, s - 1], dev_z[d])

    def kv_wait(d, w, s):
        i = zz(z - s) if d == 0 else zz(z + s)
        ref = bufs[w].at[i]
        rc(ref, ref, kvs.at[d, w, s - 1], kvr.at[d, w, s - 1], dev_z[d]).wait_recv()

    for w in range(2):
        for d in range(2):
            kv_copy(d, w, 1).start()

    factor = LOG2E * 0.125

    y_relay(1, 7, 8)
    y_relay(2, 0)
    y_send(2, 3)
    lax.fori_loop(0, 4, q_tile, 0)

    def attend(b):
        def pair(j, carry):
            cols = [pl.ds(pl.multiple_of(j * 512 + i * 256, 256), 256) for i in range(2)]
            st = [jnp.dot(kb[b], qb[:, cs], preferred_element_type=F32) for cs in cols]
            for i, cs in enumerate(cols):
                m_old = m_s[:, cs]
                m_new = jnp.maximum(m_old, jnp.max(st[i], axis=0, keepdims=True))
                p = jnp.exp2((st[i] - m_new) * factor)
                a = jnp.exp2((m_old - m_new) * factor)
                l_s[:, cs] = l_s[:, cs] * a + jnp.sum(p, axis=0, keepdims=True)
                acc_s[:, cs] = acc_s[:, cs] * a + jnp.dot(
                    vb[b], p.astype(BF16), preferred_element_type=F32
                )
                m_s[:, cs] = m_new
            return carry

        lax.fori_loop(0, 2, pair, 0)

    def conv_project():
        def tile(i, carry):
            rows = pl.ds(pl.multiple_of(i * 128, 128), 128)
            rows8 = pl.ds(pl.multiple_of(i * 128 + 8, 8), 128)
            r = jnp.dot(nrm[rows, :], w2[...].reshape(2048, 768), preferred_element_type=F32)
            postb[rows, :] = r[:, 0:256].astype(BF16)
            signal = (r[:, 256:512] * r[:, 512:768]).astype(BF16)
            sigb[rows, :] = signal
            sigf[rows8, :] = signal.astype(F32)
            return carry

        lax.fori_loop(0, 4, tile, 0)

    def halo_copy(d):
        src = sigb.at[pl.ds(496, 16)] if d == 0 else sigb.at[pl.ds(0, 16)]
        return rc(src, halo.at[d], hs.at[d], hr.at[d], dev_z[d])

    def conv_filter():
        before = halo[0].astype(F32)[8:16]
        after = halo[1].astype(F32)[0:8]
        sigf[0:8, :] = jnp.where(z > 0, before, 0.0)
        sigf[520:528, :] = jnp.where(z < NZ - 1, after, 0.0)
        taps = taps_ref[:, pl.ds(pl.multiple_of(t * 256, 256), 256)]
        for i in range(4):
            r = i * 128
            filtered = (
                taps[0:1] * sigf[r + 7 : r + 135, :]
                + taps[1:2] * sigf[r + 8 : r + 136, :]
                + taps[2:3] * sigf[r + 9 : r + 137, :]
            )
            conv[r : r + 128, :] = (
                postb[r : r + 128, :].astype(F32) * filtered
            ).astype(BF16)

    up, down = pl.ds(0, 32), pl.ds(32, 32)

    def conv_out():
        def tile(n, carry):
            cols = pl.ds(pl.multiple_of(n * 256, 256), 256)
            r = lax.dot_general(
                conv[...], w3[pl.ds(n * 2, 2)].reshape(256, 256),
                (((1,), (1,)), ((), ())), preferred_element_type=F32,
            )
            part[:, :, :, cols] = r.astype(BF16).reshape(NX, 2, 64, 256)
            return carry

        lax.fori_loop(0, 8, tile, 0)

    sums = (
        lambda: rc(part.at[:, 1 - c], pair_in, rs.at[0], rr.at[0], dev_c),
        lambda: rc(psum.at[far, up], rel.at[0], rs.at[1], rr.at[1], dev_x[0]),
        lambda: rc(psum.at[far, down], rel.at[1], rs.at[2], rr.at[2], dev_x[1]),
        lambda: rc(psum.at[right, down], fin.at[0, down], rs.at[3], rr.at[3], dev_x[0]),
        lambda: rc(psum.at[left, up], fin.at[1, up], rs.at[4], rr.at[4], dev_x[1]),
        lambda: rc(psum.at[right, up], fin.at[0, up], rs.at[5], rr.at[5], dev_x[0]),
        lambda: rc(psum.at[left, down], fin.at[1, down], rs.at[6], rr.at[6], dev_x[1]),
    )

    def sum_pair(j):
        psum[j] = (part[j, c].astype(F32) + pair_in[j].astype(F32)).astype(BF16)

    def sum_first():
        sums[0]().wait_recv()
        sum_pair(far)
        sums[1]().start()
        sums[2]().start()
        sum_pair(right)
        sum_pair(left)
        sums[3]().start()
        sums[4]().start()

    def sum_second():
        sums[1]().wait_recv()
        psum[right, 0:32] = (psum[right, 0:32].astype(F32) + rel[0].astype(F32)).astype(BF16)
        sums[5]().start()
        sums[2]().wait_recv()
        psum[left, 32:64] = (psum[left, 32:64].astype(F32) + rel[1].astype(F32)).astype(BF16)
        sums[6]().start()

    def relay(w, s):
        for d in range(2):
            kv_wait(d, w, s)
            if d == w:
                kv_copy(d, w, s + 1).start()
            else:

                @pl.when(s < 7)
                def _():
                    kv_copy(d, w, s + 1).start()

    def conv_send():
        conv_project()
        for d in range(2):
            halo_copy(d).start()

    def conv_finish():
        for d in range(2):
            halo_copy(d).wait_recv()
        conv_filter()

    def conv_sum():
        y_done(3, *range(9))
        conv_out()
        sums[0]().start()

    jobs = {
        (1, 0): lambda: (y_send(2, 4), y_relay(2, 1), y_done(1, *range(9)), a_begin()),
        (1, 1): lambda: (z_serve(6), y_relay(2, 2), y_send(2, 5)),
        (2, 0): lambda: (y_relay(2, 3),),
        (2, 1): lambda: (z_serve(7), y_send(2, 6), y_relay(2, 4)),
        (3, 0): lambda: (y_relay(2, 5),),
        (3, 1): lambda: (z_serve(8), y_send(2, 7), y_relay(2, 6), a_middle()),
        (4, 0): lambda: (y_send(2, 8), y_send(3, 0, 1, 2), y_relay(2, 7)),
        (4, 1): lambda: (y_relay(2, 8), y_send(3, 3, 4, 5, 6, 7, 8)),
        (5, 0): lambda: (y_relay(3, 0, 1, 2), a_late()),
        (5, 1): lambda: (y_relay(3, 3, 4, 5), y_done(2, *range(9)), conv_send()),
        (6, 0): lambda: (y_relay(3, 6, 7, 8),),
        (6, 1): lambda: (conv_finish(), conv_sum()),
        (7, 1): lambda: (sum_first(), a_finish()),
    }

    def serve(s, w):
        for (at, half), job in jobs.items():
            if half == w:

                @pl.when(s == at)
                def _(job=job):
                    job()

    relay(0, 1)
    jobs[1, 0]()
    relay(1, 1)
    jobs[1, 1]()
    attend(z)

    def kv_step(s, carry):
        relay(0, s)
        serve(s, 0)
        attend(zz(z - (s - 1)))
        relay(1, s)
        serve(s, 1)
        attend(zz(z + (s - 1)))
        return carry

    lax.fori_loop(2, 8, kv_step, 0)
    attend(zz(z - 7))
    attend(zz(z + 7))
    sum_second()
    kv_wait(0, 0, 8)
    kv_wait(1, 1, 8)
    attend(zz(z + 8))

    lam = lam_ref[t]
    inv = 1.0 / l_s[...]
    head = acc_s[:, 0:512] * inv[:, 0:512] - lam * (acc_s[:, 512:1024] * inv[:, 512:1024])
    r = lax.rsqrt(jnp.sum(head * head, axis=0, keepdims=True) * (1.0 / 128) + EPS)
    hid[...] = ((head * r).T * hgain_ref[...]).astype(BF16)

    def give(i):
        peer = (t + i) % 8
        rows = pl.ds(pl.multiple_of(peer * 64, 64), 64)
        return rc(hid.at[rows], ah.at[t], als.at[i - 1], alr.at[i - 1], {"tp": peer})

    for i in range(1, 8):
        give(i).start()
    ah[t] = hid[pl.ds(pl.multiple_of(t * 64, 64), 64), :]
    for k in (3, 4, 5, 6):
        sums[k]().wait_recv()
    mine = part[x, c].astype(F32) + pair_in[x].astype(F32)
    acc_o = mine + fin[0].astype(F32) + fin[1].astype(F32)
    for i in range(1, 8):
        source = (t + 8 - i) % 8
        rc(ah.at[source], ah.at[source], als.at[i - 1], alr.at[i - 1], dev_c).wait_recv()
    whole = jnp.concatenate([ah[i] for i in range(8)], axis=1)
    for n in range(8):
        w = jnp.concatenate(
            [wa[i, 2 * n : 2 * n + 2].reshape(256, 128) for i in range(8)], axis=1
        )
        r = lax.dot_general(whole, w, (((1,), (1,)), ((), ())), preferred_element_type=F32)
        cols = slice(n * 256, n * 256 + 256)
        out_ref[:, cols] = (acc_o[:, cols] + r).astype(BF16)

    for g in range(4):
        for d in range(2):
            for step in range(1, zsteps[g][d] + 1):
                z_copy(g, d, step, 2 if g < 2 and step > 1 else 1).wait_send()

    def y_drain(k, carry):
        for g in range(4):
            for d in range(2):
                y_direct(g, k, d, True).wait_send()
                y_half(g, k, d, True).wait_send()
        return carry

    lax.fori_loop(0, 16, y_drain, 0)
    for w in range(2):
        for d in range(2):
            for s in range(1, 9 if d == w else 8):
                kv_copy(d, w, s).wait_send()
    x_drain()
    a_drain()
    for d in range(2):
        halo_copy(d).wait_send()
    for make in sums:
        make().wait_send()
    for i in range(1, 8):
        give(i).wait_send()


def per_device(
    inputs, norm_gain, query_weight, key_weight, value_weight, query_gain, key_gain,
    mix_lambda, head_gain, post_gate_weight, pre_gate_weight, inner_weight, conv_taps,
    attn_out_weight, conv_out_weight,
):
    hbm = pl.BlockSpec(memory_space=pl.ANY)
    vmem = pl.BlockSpec(memory_space=pltpu.VMEM)
    smem = pl.BlockSpec(memory_space=pltpu.SMEM)
    sem = pltpu.SemaphoreType.DMA
    out = pl.pallas_call(
        body,
        out_shape=jax.ShapeDtypeStruct((64, 2048), BF16),
        in_specs=[hbm] * 9 + [vmem] * 5 + [smem],
        out_specs=vmem,
        scratch_shapes=[
            pltpu.VMEM((8, 512, 256), BF16),
            pltpu.VMEM((512, 2048), BF16),
            pltpu.VMEM((NZ, NY, 32, 384), BF16),
            pltpu.VMEM((8, NZ, NY, 32, 128), BF16),
            pltpu.VMEM((NZ, NY, 32, 768), BF16),
            pltpu.VMEM((NZ, NY, 32, 256), BF16),
            pltpu.VMEM((NZ, 512, 128), BF16),
            pltpu.VMEM((NZ, 128, 512), BF16),
            pltpu.VMEM((128, 1024), BF16),
            pltpu.VMEM((1, 1024), F32),
            pltpu.VMEM((1, 1024), F32),
            pltpu.VMEM((128, 1024), F32),
            pltpu.VMEM((512, 128), BF16),
            pltpu.VMEM((8, 64, 128), BF16),
            pltpu.VMEM((512, 256), BF16),
            pltpu.VMEM((512, 256), BF16),
            pltpu.VMEM((528, 256), F32),
            pltpu.VMEM((2, 16, 256), BF16),
            pltpu.VMEM((512, 256), BF16),
            pltpu.VMEM((NX, 2, 64, 2048), BF16),
            pltpu.VMEM((NX, 64, 2048), BF16),
            pltpu.VMEM((NX, 64, 2048), BF16),
            pltpu.VMEM((2, 32, 2048), BF16),
            pltpu.VMEM((2, 64, 2048), BF16),
            sem((9,)),
            sem((9,)),
            sem((9,)),
            sem((9,)),
            sem((9,)),
            sem((4, 2, 8)),
            sem((4, 2, 8)),
            sem((4, 2, 16)),
            sem((4, 2, 16)),
            sem((4, 2, 16)),
            sem((4, 2, 16)),
            sem((2, 2, 8)),
            sem((2, 2, 8)),
            sem((2,)),
            sem((2,)),
            sem((7,)),
            sem((7,)),
            sem((7,)),
            sem((7,)),
        ],
        compiler_params=pltpu.CompilerParams(
            collective_id=0, has_side_effects=True, vmem_limit_bytes=60 * 1024 * 1024
        ),
    )(
        inputs[0], query_weight, key_weight, value_weight, post_gate_weight,
        pre_gate_weight, inner_weight, attn_out_weight, conv_out_weight,
        norm_gain.reshape(1, -1),
        query_gain.reshape(1, -1),
        key_gain.reshape(1, -1),
        head_gain.reshape(1, -1),
        conv_taps,
        mix_lambda,
    )
    return out[None]


def solution(mesh):
    rows = P(("sp", "fs"), "tp")
    placed = (
        P("fs", "sp", "tp"), P(), rows, rows, rows, P(), P(), P(), P(),
        rows, rows, rows, P(), rows, rows,
    )
    return jax.shard_map(
        per_device,
        mesh=mesh,
        in_specs=placed,
        out_specs=P("fs", ("sp", "tp"), None),
        check_vma=False,
    )
```

time: 125 us -> 113 us (0.904)
  Pallas kernels: 121 us -> 111 us
  local copies, waits for them, and re-layouts: 3.54 us -> 1.67 us
    pallas_call x1, Pallas kernels: 121 us -> 111 us  [per_device(): pl.pallas_call(body, out_shape=jax.ShapeDtypeStruct((64, 2048), BF16), in...]
where the time goes in v2:
time: 113 us
  Pallas kernels  111 us (98%)
  local copies, waits for them, and re-layouts  1.67 us (1%)
    pallas_call x1, Pallas kernels, per_device(): pl.pallas_call(body, out_shape=jax.ShapeDtypeStruct((64, 2048), BF16), in...  111 us

profile of v2, /device:TPU:1, one launch (start us, length us, event | category | flops | bytes accessed | tf_op | source)
XLA Modules:
  0.0 113.0 jit_solution(6072280976672970806)
XLA Ops:
  0.0 111.3 %shard_map.145 = bf16[64,2048]{1,0:T(8,128)(2,1)} custom-call(bf16[512,256]{1,0:T(8,128)(2,1)} %bitcast.7, bf16[32,128]{1,0:T(8,128)(2,1)} %wq_ref.1, bf16[32,128]{1,0:T(8,128)(2,1)} %wk_ref.1, bf16[32,128]{1,0:T(8,128)(2,1)} %wv_ref.1, bf16[32,256]{1,0:T(8,128)(2,1)} %wpost_ref.1, bf16[32,256]{1,0:T(8,128)(2,1)} %wpre_ref.1, bf16[32,256]{1,0:T(8,128)(2,1)} %winner_ref.1, ...), custom_call_target="tpu_custom_call" | custom-call | tf_op jit(solution)/shard_map/pallas_call | solution.py:564
  111.3 1.7 %copy.17 = bf16[1,64,2048]{2,1,0:T(8,128)(2,1)} copy(bf16[1,64,2048]{2,1,0:T(8,128)(2,1)} %bitcast.6) | data formatting | bytes 524288
